TPU v7x, 32 devices: a whole 2x2x4 slice. The times are simulated.
32 devices in a mesh: row: 4 (over y, x), col: 8 (over z, core).
Axes of the slice: x: 2, y: 2, z: 4, core: 2. Of those that a mesh axis runs over, the one named last changes fastest.
Arguments:
- mix_input: bfloat16 [4, 4096, 512], P(None, ('row', 'col')), may hold values from -6 to 6
- group_maps: bfloat16 [4, 128, 128], replicated, may hold values from -0.5 to 0.5
- out_map: bfloat16 [512, 2048], replicated, may hold values from -0.25 to 0.25
Outputs:
- mixed: bfloat16 [4, 4096, 2048], P(None, ('row', 'col'))
All inputs are finite; a program needn't handle non-finite values.
Results may differ from a plain program's by a relative error of at most 0.011.
Values may be sent and summed in bfloat16 or wider, within the bound.
A program may use at most 64 MiB of HBM per device.

v0:
```python
import math
import jax
import jax.numpy as jnp
from jax import lax
from jax.sharding import PartitionSpec as P

precise = lax.Precision.HIGHEST


def angle_pair(left_ids, right_ids, modulus):
    turn_count = left_ids[:, None] * right_ids[None, :] % modulus
    angles = turn_count.astype(jnp.float32) * (2.0 * math.pi / modulus)
    return (jnp.cos(angles), jnp.sin(angles))


def rotate(real_part, imag_part, cosine, sine_part):
    return (real_part * cosine + imag_part * sine_part, imag_part * cosine - real_part * sine_part)


def transform(real_in, imag_in, cosine, sine_part, einsum_form):
    real_out = jnp.einsum(einsum_form, real_in, cosine, precision=precise) + jnp.einsum(
        einsum_form, imag_in, sine_part, precision=precise
    )
    imag_out = jnp.einsum(einsum_form, imag_in, cosine, precision=precise) - jnp.einsum(
        einsum_form, real_in, sine_part, precision=precise
    )
    return (real_out, imag_out)


def per_device(mix_input, group_maps, out_map):
    sequences, positions, channels = mix_input.shape
    group_count, group_width, _ = group_maps.shape
    row_count = lax.axis_size("row")
    col_count = lax.axis_size("col")
    row_id = lax.axis_index("row")
    col_id = lax.axis_index("col")
    block_span = col_count * positions
    length = row_count * block_span
    norm_factor = 1.0 / math.sqrt(length * group_width)
    width_ids = jnp.arange(group_width, dtype=jnp.int32)
    real_tab, sine_tab = angle_pair(width_ids, width_ids, group_width)
    imag_tab = -sine_tab
    lane_count = real_tab.shape[1]
    signal = mix_input.astype(jnp.float32).reshape(sequences, positions, group_count, group_width)
    real_part = jnp.einsum("spgj,jl->sglp", signal, real_tab, precision=precise)
    imag_part = jnp.einsum("spgj,jl->sglp", signal, imag_tab, precision=precise)
    total_items = sequences * group_count * lane_count
    row_items = total_items // row_count
    dev_items = row_items // col_count
    send_shape = (row_count, row_items, 1, positions)
    col_shape = (col_count, dev_items, row_count, 1, positions)
    row_ids = jnp.arange(row_count, dtype=jnp.int32)
    pos_ids = jnp.arange(positions, dtype=jnp.int32)
    col_ids = jnp.arange(col_count, dtype=jnp.int32)
    row_cos, row_sin = angle_pair(row_ids, row_ids, row_count)
    turn_cos, turn_sin = angle_pair(row_ids, col_id * positions + pos_ids, length)
    col_cos, col_sin = angle_pair(col_ids, col_ids, col_count)
    step_cos, step_sin = angle_pair(col_ids, pos_ids, block_span)
    pos_cos, pos_sin = angle_pair(pos_ids, pos_ids, positions)
    row_send = (real_part.reshape(send_shape), imag_part.reshape(send_shape))
    pieces = (
        lax.all_to_all(row_send[0], "row", split_axis=0, concat_axis=2, tiled=True),
        lax.all_to_all(row_send[1], "row", split_axis=0, concat_axis=2, tiled=True),
    )
    spun_pair = transform(pieces[0][0], pieces[1][0], row_cos, row_sin, "nrp,rk->nkp")
    real_out, imag_out = rotate(spun_pair[0], spun_pair[1], turn_cos, turn_sin)
    real_rows = real_out[None]
    imag_rows = imag_out[None]
    pieces = (
        lax.all_to_all(
            real_rows.reshape(col_shape), "col", split_axis=0, concat_axis=3, tiled=True
        ),
        lax.all_to_all(
            imag_rows.reshape(col_shape), "col", split_axis=0, concat_axis=3, tiled=True
        ),
    )
    spun_pair = transform(pieces[0][0], pieces[1][0], col_cos, col_sin, "nacp,cb->nabp")
    turned = rotate(spun_pair[0], spun_pair[1], step_cos, step_sin)
    real_out = jnp.einsum("nabp,pq->nqba", turned[0], pos_cos, precision=precise) + jnp.einsum(
        "nabp,pq->nqba", turned[1], pos_sin, precision=precise
    )
    real_spec = real_out.reshape(1, real_out.shape[0], length)
    spectrum = real_spec[0][:, None]
    spectrum = (spectrum * norm_factor).astype(jnp.bfloat16)
    halves = spectrum.shape[1]
    spectrum = spectrum.reshape(1, dev_items, halves, row_count, col_count, positions)
    returned = lax.all_to_all(spectrum, "col", split_axis=4, concat_axis=0, tiled=True)
    held_groups = sequences * group_count // row_count
    returned = returned.reshape(held_groups, lane_count, halves, row_count, positions)
    full_width = returned[:, :, 0]
    group_ids = (row_id * held_groups + jnp.arange(held_groups, dtype=jnp.int32)) % group_count
    picker = (group_ids[:, None] == jnp.arange(group_count, dtype=jnp.int32)[None, :]).astype(
        jnp.bfloat16
    )
    chosen = jnp.einsum(
        "hg,glm->hlm", picker, group_maps, preferred_element_type=jnp.float32
    ).astype(jnp.bfloat16)
    grouped = jnp.einsum(
        "hlap,hlm->hapm", full_width, chosen, preferred_element_type=jnp.float32
    ).astype(jnp.bfloat16)
    grouped = grouped.reshape(1, held_groups, row_count, positions, group_width)
    arrived = lax.all_to_all(grouped, "row", split_axis=2, concat_axis=0, tiled=True)
    arrived = arrived.reshape(sequences, group_count, positions, group_width)
    mixed_out = jnp.einsum(
        "sgpm,gmn->spn",
        arrived,
        out_map.reshape(group_count, group_width, out_map.shape[1]),
        preferred_element_type=jnp.float32,
    )
    return mixed_out.astype(jnp.bfloat16)


def solution(mesh):
    return jax.shard_map(
        per_device,
        mesh=mesh,
        in_specs=(P(None, ("row", "col"), None), P(), P()),
        out_specs=P(None, ("row", "col"), None),
        check_vma=False,
    )
```

profile of v0, /device:TPU:0, one launch (start us, length us, event | category | flops | bytes accessed | tf_op | source)
XLA Modules:
  0.0 157.9 jit_solution(9652048484400523859)
XLA Ops:
  0.0 0.0 copy-start
  0.0 3.0 %fusion.30 = f32[128,4,128,4]{2,0,3,1:T(8,128)} fusion(bf16[4,128,512]{2,1,0:T(8,128)(2,1)} %param.3), kind=kOutput, calls=%fused_computation.42 | convolution fusion | flops 402882560 | bytes 1572864 | tf_op jit(solution)/shard_map/spgj,jl->sglp/dot_general | solution.py:45
  3.0 5.2 %all-to-all-start = ((f32[4,512,1,128]{3,1,2,0:T(8,128)}), f32[4,512,1,128]{3,1,2,0:T(8,128)S(1)}, u32[]{:S(2)}, u32[]{:S(2)}) async-start(f32[4,512,1,128]{3,1,2,0:T(8,128)} %bitcast.153), calls=%async_computation | async-start | bytes 2097152 | tf_op jit(solution)/shard_map/all_to_all | solution.py:62
  8.2 2.9 %fusion.28 = f32[128,4,128,4]{2,0,3,1:T(8,128)} fusion(bf16[4,128,512]{2,1,0:T(8,128)(2,1)} %param.3), kind=kOutput, calls=%fused_computation.40 | convolution fusion | flops 402898944 | bytes 1572864 | tf_op jit(solution)/shard_map/spgj,jl->sglp/dot_general | solution.py:46
  11.1 10.7 %all-to-all-done = f32[4,512,1,128]{3,1,2,0:T(8,128)S(1)} async-done(((f32[4,512,1,128]{3,1,2,0:T(8,128)}), f32[4,512,1,128]{3,1,2,0:T(8,128)S(1)}, u32[]{:S(2)}, u32[]{:S(2)}) %all-to-all-start) | async-done | bytes 1048608 | tf_op jit(solution)/shard_map/all_to_all | solution.py:62
  21.8 1.0 copy-done.1
  22.8 3.5 %all-to-all-start.1 = ((f32[4,512,1,128]{3,1,2,0:T(8,128)}), f32[4,512,1,128]{3,1,2,0:T(8,128)S(1)}, u32[]{:S(2)}, u32[]{:S(2)}) async-start(f32[4,512,1,128]{3,1,2,0:T(8,128)} %bitcast.152), calls=%async_computation.1 | async-start | bytes 2097152 | tf_op jit(solution)/shard_map/all_to_all | solution.py:63
  26.3 0.1 fusion.94
  26.4 4.6 %fusion.12 = f32[4,512,128]{2,0,1:T(4,128)} fusion(f32[4,512,1,128]{3,1,2,0:T(8,128)} %copy-done.1), kind=kOutput, calls=%fused_computation.20 | convolution fusion | flops 12583136 | bytes 2097152 | tf_op jit(solution)/shard_map/nrp,rk->nkp/dot_general | solution.py:21
  31.0 8.5 %all-to-all-done.1 = f32[4,512,1,128]{3,1,2,0:T(8,128)S(1)} async-done(((f32[4,512,1,128]{3,1,2,0:T(8,128)}), f32[4,512,1,128]{3,1,2,0:T(8,128)S(1)}, u32[]{:S(2)}, u32[]{:S(2)}) %all-to-all-start.1) | async-done | bytes 1048608 | tf_op jit(solution)/shard_map/all_to_all | solution.py:63
  39.5 2.4 %fusion.14 = f32[4,512,128]{2,0,1:T(4,128)S(1)} fusion(f32[4,512,1,128]{3,1,2,0:T(8,128)S(1)} %all-to-all-done.1), kind=kOutput, calls=%fused_computation.22 | convolution fusion | flops 12583136 | bytes 2097152 | tf_op jit(solution)/shard_map/nrp,rk->nkp/dot_general | solution.py:24
  41.8 0.0 copy-start.2
  41.8 2.5 %convolution_add_fusion.2 = f32[4,512,128]{2,0,1:T(4,128)S(1)} fusion(f32[4,512,128]{2,0,1:T(4,128)S(1)} %copy-done.3, f32[4,512,1,128]{3,1,2,0:T(8,128)S(1)} %all-to-all-done.1), kind=kOutput, calls=%fused_computation.6 | convolution fusion | flops 12845280 | bytes 3145728 | tf_op jit(solution)/shard_map/nrp,rk->nkp/dot_general | solution.py:21
  44.4 3.9 %multiply_add_fusion = (f32[4,512,128]{2,0,1:T(4,128)}, f32[4,512,128]{2,0,1:T(4,128)S(1)}) fusion(f32[4,512,128]{2,0,1:T(4,128)S(1)} %convolution_add_fusion.2, f32[4,128]{1,0:T(4,128)S(1)} %get-tuple-element.10, f32[4,128]{1,0:T(4,128)S(1)} %get-tuple-element.9, f32[4,512,128]{2,0,1:T(4,128)S(1)} %fusion.14, f32[4,512,1,128]{3,1,2,0:T(8,128)S(1)} %copy-done.2), kind=kOutput, calls=%fused_computation.31 | convolution fusion | flops 14418144 | bytes 5246976 | tf_op jit(solution)/shard_map/nrp,rk->nkp/dot_general | solution.py:24
  48.3 31.3 %all_to_all.90 = f32[8,64,4,1,128]{4,2,1,3,0:T(4,128)S(1)} all-to-all(f32[8,64,4,1,128]{4,2,1,3,0:T(4,128)S(1)} %bitcast.155), channel_id=1, replica_groups=mesh['row'=4,'col'=8] {'col'}, dimensions={0} | all-to-all | bytes 2097152 | tf_op jit(solution)/shard_map/all_to_all | solution.py:73
  79.5 4.4 %all-to-all-start.2 = ((f32[8,64,4,1,128]{4,2,1,3,0:T(4,128)}), f32[8,64,4,1,128]{4,2,1,3,0:T(4,128)}, u32[]{:S(2)}, u32[]{:S(2)}) async-start(f32[8,64,4,1,128]{4,2,1,3,0:T(4,128)} %bitcast.154), calls=%async_computation.2 | async-start | bytes 2097152 | tf_op jit(solution)/shard_map/all_to_all | solution.py:70
  84.0 0.1 fusion.82
  84.0 2.5 %fusion.8 = f32[8,64,4,128]{3,0,2,1:T(8,128)} fusion(f32[8,64,4,1,128]{4,2,1,3,0:T(4,128)S(1)} %all_to_all.90), kind=kOutput, calls=%fused_computation.16 | convolution fusion | flops 25166720 | bytes 2097152 | tf_op jit(solution)/shard_map/nacp,cb->nabp/dot_general | solution.py:24
  86.5 23.8 %all-to-all-done.2 = f32[8,64,4,1,128]{4,2,1,3,0:T(4,128)} async-done(((f32[8,64,4,1,128]{4,2,1,3,0:T(4,128)}), f32[8,64,4,1,128]{4,2,1,3,0:T(4,128)}, u32[]{:S(2)}, u32[]{:S(2)}) %all-to-all-start.2) | async-done | bytes 1048608 | tf_op jit(solution)/shard_map/all_to_all | solution.py:70
  110.4 2.8 %fusion.6 = f32[8,64,4,128]{3,0,2,1:T(8,128)S(1)} fusion(f32[8,64,4,1,128]{4,2,1,3,0:T(4,128)} %all-to-all-done.2), kind=kOutput, calls=%fused_computation.14 | convolution fusion | flops 25166720 | bytes 2097152 | tf_op jit(solution)/shard_map/nacp,cb->nabp/dot_general | solution.py:21
  113.2 2.7 %convolution_subtract_fusion = f32[8,64,4,128]{3,0,2,1:T(8,128)S(1)} fusion(f32[8,64,4,128]{3,0,2,1:T(8,128)S(1)} %copy-done.4, f32[8,64,4,1,128]{4,2,1,3,0:T(4,128)} %all-to-all-done.2), kind=kOutput, calls=%fused_computation.3 | convolution fusion | flops 25428864 | bytes 3145728 | tf_op jit(solution)/shard_map/nacp,cb->nabp/dot_general | solution.py:24
  115.9 1.7 %subtract_bitcast_fusion = (f32[64,4,8,128]{3,2,1,0:T(8,128)S(1)}, f32[64,4,8,128]{3,2,1,0:T(8,128)S(1)}) fusion(f32[8,64,4,128]{3,0,2,1:T(8,128)S(1)} %convolution_subtract_fusion, f32[8,128]{1,0:T(8,128)S(1)} %get-tuple-element.11, f32[8,128]{1,0:T(8,128)S(1)} %get-tuple-element.12, f32[8,64,4,128]{3,0,2,1:T(8,128)S(1)} %fusion.6, ...), kind=kOutput, calls=%fused_computation.28 | convolution fusion | flops 27001728 | bytes 5251072 | tf_op jit(solution)/shard_map/nacp,cb->nabp/dot_general | solution.py:21
  117.7 1.9 %fusion.18 = f32[128,64,4,8]{0,1,3,2:T(8,128)S(1)} fusion(f32[64,4,8,128]{3,2,1,0:T(8,128)S(1)} %get-tuple-element.6), kind=kOutput, calls=%fused_computation.26 | convolution fusion | flops 402882560 | bytes 2097152 | tf_op jit(solution)/shard_map/nabp,pq->nqba/dot_general | solution.py:79
  119.5 2.7 %fusion.3 = bf16[64,128,8,4]{1,0,2,3:T(8,128)(2,1)} fusion(f32[128,64,4,8]{0,1,3,2:T(8,128)S(1)} %fusion.18, f32[64,4,8,128]{3,2,1,0:T(8,128)S(1)} %get-tuple-element.5), kind=kOutput, calls=%fused_computation.10 | convolution fusion | flops 403668992 | bytes 2621440 | tf_op jit(solution)/shard_map/nabp,pq->nqba/dot_general | solution.py:79
  122.2 1.9 %copy.43 = bf16[64,128,8,4]{0,3,2,1:T(4,128)(2,1)S(1)} copy(bf16[64,128,8,4]{1,0,2,3:T(8,128)(2,1)} %fusion.3) | data formatting | bytes 1048576 | tf_op jit(solution)/shard_map/convert_element_type | solution.py:84
  124.1 1.1 copy.44
  125.2 3.5 %all-to-all-start.4 = ((bf16[1,64,1,4,8,128]{5,1,3,2,0,4:T(8,128)(2,1)}), bf16[1,64,1,4,8,128]{5,1,3,2,0,4:T(8,128)(2,1)S(1)}, u32[]{:S(2)}, u32[]{:S(2)}) async-start(bf16[1,64,1,4,8,128]{5,1,3,2,0,4:T(8,128)(2,1)} %copy.44), calls=%async_computation.4 | async-start | bytes 1048576 | tf_op jit(solution)/shard_map/all_to_all | solution.py:87
  128.7 0.3 fusion.4
  129.0 14.9 %all-to-all-done.4 = bf16[1,64,1,4,8,128]{5,1,3,2,0,4:T(8,128)(2,1)S(1)} async-done(((bf16[1,64,1,4,8,128]{5,1,3,2,0,4:T(8,128)(2,1)}), bf16[1,64,1,4,8,128]{5,1,3,2,0,4:T(8,128)(2,1)S(1)}, u32[]{:S(2)}, u32[]{:S(2)}) %all-to-all-start.4) | async-done | bytes 524320 | tf_op jit(solution)/shard_map/all_to_all | solution.py:87
  144.0 0.4 fusion.2
  144.4 10.9 %all_to_all.91 = bf16[1,4,4,128,128]{4,3,1,0,2:T(8,128)(2,1)S(1)} all-to-all(bf16[1,4,4,128,128]{4,3,1,0,2:T(8,128)(2,1)S(1)} %copy.49), channel_id=1, replica_groups=mesh['row'=4,'col'=8] {'row'}, dimensions={2} | all-to-all | bytes 1048576 | tf_op jit(solution)/shard_map/all_to_all | solution.py:102
  155.3 2.6 %bitcast_convert_fusion = bf16[4,128,2048]{2,1,0:T(8,128)(2,1)} fusion(bf16[4,128,2048,1]{2,1,3,0:T(8,128)(2,1)S(1)} %bitcast.150, bf16[1,4,4,128,128]{4,3,1,0,2:T(8,128)(2,1)S(1)} %all_to_all.91), kind=kOutput, calls=%fused_computation | convolution fusion | flops 1074790400 | bytes 4718592 | tf_op jit(solution)/shard_map/sgpm,gmn->spn/dot_general | solution.py:104
  (13 shorter events, 0.1 us)
Async XLA Ops:
  0.0 155.3 %copy-start = (bf16[512,2048]{1,0:T(8,128)(2,1)S(1)}, bf16[512,2048]{1,0:T(8,128)(2,1)}, u32[]{:S(2)}) copy-start(bf16[512,2048]{1,0:T(8,128)(2,1)} %param.5) | copy-start | bytes 6291460
  3.0 18.8 %all-to-all-start = ((f32[4,512,1,128]{3,1,2,0:T(8,128)}), f32[4,512,1,128]{3,1,2,0:T(8,128)S(1)}, u32[]{:S(2)}, u32[]{:S(2)}) async-start(f32[4,512,1,128]{3,1,2,0:T(8,128)} %bitcast.153), calls=%async_computation | async-start | bytes 2097152 | tf_op jit(solution)/shard_map/all_to_all | solution.py:62
  21.8 1.0 copy-start.1
  22.8 16.6 %all-to-all-start.1 = ((f32[4,512,1,128]{3,1,2,0:T(8,128)}), f32[4,512,1,128]{3,1,2,0:T(8,128)S(1)}, u32[]{:S(2)}, u32[]{:S(2)}) async-start(f32[4,512,1,128]{3,1,2,0:T(8,128)} %bitcast.152), calls=%async_computation.1 | async-start | bytes 2097152 | tf_op jit(solution)/shard_map/all_to_all | solution.py:63
  39.5 2.4 %copy-start.3 = (f32[4,512,128]{2,0,1:T(4,128)S(1)}, f32[4,512,128]{2,0,1:T(4,128)}, u32[]{:S(2)}) copy-start(f32[4,512,128]{2,0,1:T(4,128)} %fusion.12) | copy-start | bytes 3145732
  41.8 2.5 %copy-start.2 = (f32[4,512,1,128]{3,1,2,0:T(8,128)S(1)}, f32[4,512,1,128]{3,1,2,0:T(8,128)}, u32[]{:S(2)}) copy-start(f32[4,512,1,128]{3,1,2,0:T(8,128)} %copy-done.1) | copy-start | bytes 3145732
  79.5 30.8 %all-to-all-start.2 = ((f32[8,64,4,1,128]{4,2,1,3,0:T(4,128)}), f32[8,64,4,1,128]{4,2,1,3,0:T(4,128)}, u32[]{:S(2)}, u32[]{:S(2)}) async-start(f32[8,64,4,1,128]{4,2,1,3,0:T(4,128)} %bitcast.154), calls=%async_computation.2 | async-start | bytes 2097152 | tf_op jit(solution)/shard_map/all_to_all | solution.py:70
  110.4 2.8 %copy-start.4 = (f32[8,64,4,128]{3,0,2,1:T(8,128)S(1)}, f32[8,64,4,128]{3,0,2,1:T(8,128)}, u32[]{:S(2)}) copy-start(f32[8,64,4,128]{3,0,2,1:T(8,128)} %fusion.8) | copy-start | bytes 3145732
  122.2 6.5 %copy-start.5 = (bf16[4,128,128]{2,1,0:T(8,128)(2,1)S(1)}, bf16[4,128,128]{2,1,0:T(8,128)(2,1)}, u32[]{:S(2)}) copy-start(bf16[4,128,128]{2,1,0:T(8,128)(2,1)} %param.4) | copy-start | bytes 393220
  125.2 18.8 %all-to-all-start.4 = ((bf16[1,64,1,4,8,128]{5,1,3,2,0,4:T(8,128)(2,1)}), bf16[1,64,1,4,8,128]{5,1,3,2,0,4:T(8,128)(2,1)S(1)}, u32[]{:S(2)}, u32[]{:S(2)}) async-start(bf16[1,64,1,4,8,128]{5,1,3,2,0,4:T(8,128)(2,1)} %copy.44), calls=%async_computation.4 | async-start | bytes 1048576 | tf_op jit(solution)/shard_map/all_to_all | solution.py:87
where the time goes:
time: 159 us; the launch traced here: 158 us
  waiting for transfers between devices  58 us (36%)
  blocking collectives  42.2 us (27%)
  matrix products  36.8 us (23%)
  starting transfers between devices  16.6 us (10%)
  local copies, waits for them, and re-layouts  4.07 us (3%)
    all_to_all x1, blocking collectives, per_device(): lax.all_to_all(imag_rows.reshape(col_shape), 'col', split_axis=0, concat_...  31.3 us
    all_to_all x1, waiting for transfers between devices, per_device(): lax.all_to_all(real_rows.reshape(col_shape), 'col', split_axis=0, concat_...  23.8 us
    all_to_all x1, waiting for transfers between devices, per_device(): lax.all_to_all(spectrum, 'col', split_axis=4, concat_axis=0, tiled=True)  14.9 us
    all_to_all x1, blocking collectives, per_device(): lax.all_to_all(grouped, 'row', split_axis=2, concat_axis=0, tiled=True)  10.9 us
    all_to_all x1, waiting for transfers between devices, per_device(): lax.all_to_all(row_send[0], 'row', split_axis=0, concat_axis=2, tiled=True)  10.7 us
    all_to_all x1, waiting for transfers between devices, per_device(): lax.all_to_all(row_send[1], 'row', split_axis=0, concat_axis=2, tiled=True)  8.48 us
    dot_general x2, matrix products, transform(): jnp.einsum(einsum_form, real_in, cosine, precision=precise)  7.38 us
    dot_general x2, matrix products, transform(): jnp.einsum(einsum_form, real_in, sine_part, precision=precise)  6.61 us
  transfers between devices with their start and end apart: 4, of which 4 were waited for; matrix products, arithmetic and copies ran while one was open for 7% of the time, Pallas kernels for 0%

commit v1 on v0

--- a/solution.py
+++ b/solution.py
@@ -84,7 +84,10 @@
     spectrum = (spectrum * norm_factor).astype(jnp.bfloat16)
     halves = spectrum.shape[1]
     spectrum = spectrum.reshape(1, dev_items, halves, row_count, col_count, positions)
-    returned = lax.all_to_all(spectrum, "col", split_axis=4, concat_axis=0, tiled=True)
+    returned = jnp.concatenate(
+        lax.all_to_all(jnp.stack(jnp.split(spectrum, lax.axis_size("col"), axis=4)), "col", 0, 0),
+        axis=0,
+    )
     held_groups = sequences * group_count // row_count
     returned = returned.reshape(held_groups, lane_count, halves, row_count, positions)
     full_width = returned[:, :, 0]

time: 159 us -> 165 us (1.038)
  local copies, waits for them, and re-layouts: 4.07 us -> 10.6 us
    unnamed x12 -> x19, local copies, waits for them, and re-layouts: 0.99 us -> 5.64 us
    another operation x0 -> x2, local copies, waits for them, and re-layouts: none -> 3 us  [per_device(): jnp.stack(jnp.split(spectrum, lax.axis_size('col'), axis=4))]
  transfers between devices with their start and end apart: 4 -> 4, of which waited for: 4 -> 4; matrix products, arithmetic and copies ran while one was open for 7% -> 6% of each run, Pallas kernels for 0% -> 0%
where the time goes in v1:
time: 165 us; the launch traced here: 164 us
  waiting for transfers between devices  58 us (35%)
  blocking collectives  42.2 us (26%)
  matrix products  36.8 us (22%)
  starting transfers between devices  16.6 us (10%)
  local copies, waits for them, and re-layouts  10.6 us (6%)
    all_to_all x1, blocking collectives, per_device(): lax.all_to_all(imag_rows.reshape(col_shape), 'col', split_axis=0, concat_...  31.3 us
    all_to_all x1, waiting for transfers between devices, per_device(): lax.all_to_all(real_rows.reshape(col_shape), 'col', split_axis=0, concat_...  23.8 us
    all_to_all x1, waiting for transfers between devices, per_device(): lax.all_to_all(jnp.stack(jnp.split(spectrum, lax.axis_size('col'), axis=4...  14.9 us
    all_to_all x1, blocking collectives, per_device(): lax.all_to_all(grouped, 'row', split_axis=2, concat_axis=0, tiled=True)  10.9 us
    all_to_all x1, waiting for transfers between devices, per_device(): lax.all_to_all(row_send[0], 'row', split_axis=0, concat_axis=2, tiled=True)  10.7 us
    all_to_all x1, waiting for transfers between devices, per_device(): lax.all_to_all(row_send[1], 'row', split_axis=0, concat_axis=2, tiled=True)  8.48 us
    dot_general x2, matrix products, transform(): jnp.einsum(einsum_form, real_in, cosine, precision=precise)  7.38 us
    dot_general x2, matrix products, transform(): jnp.einsum(einsum_form, real_in, sine_part, precision=precise)  6.61 us
  transfers between devices with their start and end apart: 4, of which 4 were waited for; matrix products, arithmetic and copies ran while one was open for 6% of the time, Pallas kernels for 0%

profile of v1, /device:TPU:0, one launch (start us, length us, event | category | flops | bytes accessed | tf_op | source)
XLA Modules:
  0.0 164.4 jit_solution(14262760907626819341)
XLA Ops:
  0.0 3.0 %fusion.30 = f32[128,4,128,4]{2,0,3,1:T(8,128)} fusion(bf16[4,128,512]{2,1,0:T(8,128)(2,1)} %param.3), kind=kOutput, calls=%fused_computation.42 | convolution fusion | flops 402882560 | bytes 1572864 | tf_op jit(solution)/shard_map/spgj,jl->sglp/dot_general | solution.py:45
  3.0 5.2 %all-to-all-start = ((f32[4,512,1,128]{3,1,2,0:T(8,128)}), f32[4,512,1,128]{3,1,2,0:T(8,128)S(1)}, u32[]{:S(2)}, u32[]{:S(2)}) async-start(f32[4,512,1,128]{3,1,2,0:T(8,128)} %bitcast.200), calls=%async_computation | async-start | bytes 2097152 | tf_op jit(solution)/shard_map/all_to_all | solution.py:62
  8.2 2.9 %fusion.28 = f32[128,4,128,4]{2,0,3,1:T(8,128)} fusion(bf16[4,128,512]{2,1,0:T(8,128)(2,1)} %param.3), kind=kOutput, calls=%fused_computation.40 | convolution fusion | flops 402898944 | bytes 1572864 | tf_op jit(solution)/shard_map/spgj,jl->sglp/dot_general | solution.py:46
  11.1 10.7 %all-to-all-done = f32[4,512,1,128]{3,1,2,0:T(8,128)S(1)} async-done(((f32[4,512,1,128]{3,1,2,0:T(8,128)}), f32[4,512,1,128]{3,1,2,0:T(8,128)S(1)}, u32[]{:S(2)}, u32[]{:S(2)}) %all-to-all-start) | async-done | bytes 1048608 | tf_op jit(solution)/shard_map/all_to_all | solution.py:62
  21.8 1.0 copy-done.1
  22.8 3.5 %all-to-all-start.1 = ((f32[4,512,1,128]{3,1,2,0:T(8,128)}), f32[4,512,1,128]{3,1,2,0:T(8,128)S(1)}, u32[]{:S(2)}, u32[]{:S(2)}) async-start(f32[4,512,1,128]{3,1,2,0:T(8,128)} %bitcast.199), calls=%async_computation.1 | async-start | bytes 2097152 | tf_op jit(solution)/shard_map/all_to_all | solution.py:63
  26.4 4.6 %fusion.12 = f32[4,512,128]{2,0,1:T(4,128)} fusion(f32[4,512,1,128]{3,1,2,0:T(8,128)} %copy-done.1), kind=kOutput, calls=%fused_computation.20 | convolution fusion | flops 12583136 | bytes 2097152 | tf_op jit(solution)/shard_map/nrp,rk->nkp/dot_general | solution.py:21
  31.0 8.5 %all-to-all-done.1 = f32[4,512,1,128]{3,1,2,0:T(8,128)S(1)} async-done(((f32[4,512,1,128]{3,1,2,0:T(8,128)}), f32[4,512,1,128]{3,1,2,0:T(8,128)S(1)}, u32[]{:S(2)}, u32[]{:S(2)}) %all-to-all-start.1) | async-done | bytes 1048608 | tf_op jit(solution)/shard_map/all_to_all | solution.py:63
  39.5 2.4 %fusion.14 = f32[4,512,128]{2,0,1:T(4,128)S(1)} fusion(f32[4,512,1,128]{3,1,2,0:T(8,128)S(1)} %all-to-all-done.1), kind=kOutput, calls=%fused_computation.22 | convolution fusion | flops 12583136 | bytes 2097152 | tf_op jit(solution)/shard_map/nrp,rk->nkp/dot_general | solution.py:24
  41.8 2.5 %convolution_add_fusion.2 = f32[4,512,128]{2,0,1:T(4,128)S(1)} fusion(f32[4,512,128]{2,0,1:T(4,128)S(1)} %copy-done.3, f32[4,512,1,128]{3,1,2,0:T(8,128)S(1)} %all-to-all-done.1), kind=kOutput, calls=%fused_computation.6 | convolution fusion | flops 12845280 | bytes 3145728 | tf_op jit(solution)/shard_map/nrp,rk->nkp/dot_general | solution.py:21
  44.4 3.9 %multiply_add_fusion = (f32[4,512,128]{2,0,1:T(4,128)}, f32[4,512,128]{2,0,1:T(4,128)S(1)}) fusion(f32[4,512,128]{2,0,1:T(4,128)S(1)} %convolution_add_fusion.2, f32[4,128]{1,0:T(4,128)S(1)} %get-tuple-element.10, f32[4,128]{1,0:T(4,128)S(1)} %get-tuple-element.9, f32[4,512,128]{2,0,1:T(4,128)S(1)} %fusion.14, f32[4,512,1,128]{3,1,2,0:T(8,128)S(1)} %copy-done.2), kind=kOutput, calls=%fused_computation.31 | convolution fusion | flops 14418144 | bytes 5246976 | tf_op jit(solution)/shard_map/nrp,rk->nkp/dot_general | solution.py:24
  48.3 31.3 %all_to_all.80 = f32[8,64,4,1,128]{4,2,1,3,0:T(4,128)S(1)} all-to-all(f32[8,64,4,1,128]{4,2,1,3,0:T(4,128)S(1)} %bitcast.202), channel_id=1, replica_groups=mesh['row'=4,'col'=8] {'col'}, dimensions={0} | all-to-all | bytes 2097152 | tf_op jit(solution)/shard_map/all_to_all | solution.py:73
  79.5 4.4 %all-to-all-start.2 = ((f32[8,64,4,1,128]{4,2,1,3,0:T(4,128)}), f32[8,64,4,1,128]{4,2,1,3,0:T(4,128)}, u32[]{:S(2)}, u32[]{:S(2)}) async-start(f32[8,64,4,1,128]{4,2,1,3,0:T(4,128)} %bitcast.201), calls=%async_computation.2 | async-start | bytes 2097152 | tf_op jit(solution)/shard_map/all_to_all | solution.py:70
  84.0 2.5 %fusion.8 = f32[8,64,4,128]{3,0,2,1:T(8,128)} fusion(f32[8,64,4,1,128]{4,2,1,3,0:T(4,128)S(1)} %all_to_all.80), kind=kOutput, calls=%fused_computation.16 | convolution fusion | flops 25166720 | bytes 2097152 | tf_op jit(solution)/shard_map/nacp,cb->nabp/dot_general | solution.py:24
  86.5 23.8 %all-to-all-done.2 = f32[8,64,4,1,128]{4,2,1,3,0:T(4,128)} async-done(((f32[8,64,4,1,128]{4,2,1,3,0:T(4,128)}), f32[8,64,4,1,128]{4,2,1,3,0:T(4,128)}, u32[]{:S(2)}, u32[]{:S(2)}) %all-to-all-start.2) | async-done | bytes 1048608 | tf_op jit(solution)/shard_map/all_to_all | solution.py:70
  110.4 2.8 %fusion.6 = f32[8,64,4,128]{3,0,2,1:T(8,128)S(1)} fusion(f32[8,64,4,1,128]{4,2,1,3,0:T(4,128)} %all-to-all-done.2), kind=kOutput, calls=%fused_computation.14 | convolution fusion | flops 25166720 | bytes 2097152 | tf_op jit(solution)/shard_map/nacp,cb->nabp/dot_general | solution.py:21
  113.2 2.7 %convolution_subtract_fusion = f32[8,64,4,128]{3,0,2,1:T(8,128)S(1)} fusion(f32[8,64,4,128]{3,0,2,1:T(8,128)S(1)} %copy-done.4, f32[8,64,4,1,128]{4,2,1,3,0:T(4,128)} %all-to-all-done.2), kind=kOutput, calls=%fused_computation.3 | convolution fusion | flops 25428864 | bytes 3145728 | tf_op jit(solution)/shard_map/nacp,cb->nabp/dot_general | solution.py:24
  115.9 1.7 %subtract_bitcast_fusion = (f32[64,4,8,128]{3,2,1,0:T(8,128)S(1)}, f32[64,4,8,128]{3,2,1,0:T(8,128)S(1)}) fusion(f32[8,64,4,128]{3,0,2,1:T(8,128)S(1)} %convolution_subtract_fusion, f32[8,128]{1,0:T(8,128)S(1)} %get-tuple-element.11, f32[8,128]{1,0:T(8,128)S(1)} %get-tuple-element.12, f32[8,64,4,128]{3,0,2,1:T(8,128)S(1)} %fusion.6, ...), kind=kOutput, calls=%fused_computation.28 | convolution fusion | flops 27001728 | bytes 5251072 | tf_op jit(solution)/shard_map/nacp,cb->nabp/dot_general | solution.py:21
  117.7 1.9 %fusion.18 = f32[128,64,4,8]{0,1,3,2:T(8,128)S(1)} fusion(f32[64,4,8,128]{3,2,1,0:T(8,128)S(1)} %get-tuple-element.6), kind=kOutput, calls=%fused_computation.26 | convolution fusion | flops 402882560 | bytes 2097152 | tf_op jit(solution)/shard_map/nabp,pq->nqba/dot_general | solution.py:79
  119.5 2.7 %fusion.3 = bf16[64,128,8,4]{1,0,2,3:T(8,128)(2,1)} fusion(f32[128,64,4,8]{0,1,3,2:T(8,128)S(1)} %fusion.18, f32[64,4,8,128]{3,2,1,0:T(8,128)S(1)} %get-tuple-element.5), kind=kOutput, calls=%fused_computation.10 | convolution fusion | flops 403668992 | bytes 2621440 | tf_op jit(solution)/shard_map/nabp,pq->nqba/dot_general | solution.py:79
  122.2 1.8 %copy.58 = bf16[64,128,8,4]{0,3,2,1:T(4,128)(2,1)S(1)} copy(bf16[64,128,8,4]{1,0,2,3:T(8,128)(2,1)} %fusion.3) | data formatting | bytes 1048576 | tf_op jit(solution)/shard_map/convert_element_type | solution.py:84
  124.0 0.7 fusion.44
  124.7 0.7 fusion.43
  125.4 0.7 fusion.42
  126.0 0.7 fusion.41
  127.4 0.7 fusion.39
  128.7 0.7 fusion.37
  129.4 2.3 %copy.67 = bf16[8,1,64,1,4,1,128]{6,2,5,4,3,1,0:T(8,128)(2,1)} copy(bf16[8,1,64,1,4,1,128]{2,6,4,5,3,1,0:T(8,128)(2,1)} %fusion.37) | data formatting | bytes 1048576 | tf_op jit(solution)/shard_map/stack | solution.py:88
  131.7 3.5 %all-to-all-start.4 = ((bf16[8,1,64,1,4,1,128]{6,2,5,4,3,1,0:T(8,128)(2,1)}), bf16[8,1,64,1,4,1,128]{6,2,5,4,3,1,0:T(8,128)(2,1)S(1)}, u32[]{:S(2)}, u32[]{:S(2)}) async-start(bf16[8,1,64,1,4,1,128]{6,2,5,4,3,1,0:T(8,128)(2,1)} %copy.67), calls=%async_computation.4 | async-start | bytes 1048576 | tf_op jit(solution)/shard_map/all_to_all | solution.py:88
  135.5 14.9 %all-to-all-done.4 = bf16[8,1,64,1,4,1,128]{6,2,5,4,3,1,0:T(8,128)(2,1)S(1)} async-done(((bf16[8,1,64,1,4,1,128]{6,2,5,4,3,1,0:T(8,128)(2,1)}), bf16[8,1,64,1,4,1,128]{6,2,5,4,3,1,0:T(8,128)(2,1)S(1)}, u32[]{:S(2)}, u32[]{:S(2)}) %all-to-all-start.4) | async-done | bytes 524320 | tf_op jit(solution)/shard_map/all_to_all | solution.py:88
  150.9 10.9 %all_to_all.81 = bf16[1,4,4,128,128]{4,3,1,0,2:T(8,128)(2,1)S(1)} all-to-all(bf16[1,4,4,128,128]{4,3,1,0,2:T(8,128)(2,1)S(1)} %copy.72), channel_id=1, replica_groups=mesh['row'=4,'col'=8] {'row'}, dimensions={2} | all-to-all | bytes 1048576 | tf_op jit(solution)/shard_map/all_to_all | solution.py:105
  161.8 2.6 %bitcast_convert_fusion = bf16[4,128,2048]{2,1,0:T(8,128)(2,1)} fusion(bf16[4,128,2048,1]{2,1,3,0:T(8,128)(2,1)S(1)} %bitcast.190, bf16[1,4,4,128,128]{4,3,1,0,2:T(8,128)(2,1)S(1)} %all_to_all.81), kind=kOutput, calls=%fused_computation | convolution fusion | flops 1074790400 | bytes 4718592 | tf_op jit(solution)/shard_map/sgpm,gmn->spn/dot_general | solution.py:107
  (21 shorter events, 2.2 us)
Async XLA Ops:
  0.0 161.8 %copy-start = (bf16[512,2048]{1,0:T(8,128)(2,1)S(1)}, bf16[512,2048]{1,0:T(8,128)(2,1)}, u32[]{:S(2)}) copy-start(bf16[512,2048]{1,0:T(8,128)(2,1)} %param.5) | copy-start | bytes 6291460
  3.0 18.8 %all-to-all-start = ((f32[4,512,1,128]{3,1,2,0:T(8,128)}), f32[4,512,1,128]{3,1,2,0:T(8,128)S(1)}, u32[]{:S(2)}, u32[]{:S(2)}) async-start(f32[4,512,1,128]{3,1,2,0:T(8,128)} %bitcast.200), calls=%async_computation | async-start | bytes 2097152 | tf_op jit(solution)/shard_map/all_to_all | solution.py:62
  21.8 1.0 copy-start.1
  22.8 16.6 %all-to-all-start.1 = ((f32[4,512,1,128]{3,1,2,0:T(8,128)}), f32[4,512,1,128]{3,1,2,0:T(8,128)S(1)}, u32[]{:S(2)}, u32[]{:S(2)}) async-start(f32[4,512,1,128]{3,1,2,0:T(8,128)} %bitcast.199), calls=%async_computation.1 | async-start | bytes 2097152 | tf_op jit(solution)/shard_map/all_to_all | solution.py:63
  39.5 2.4 %copy-start.3 = (f32[4,512,128]{2,0,1:T(4,128)S(1)}, f32[4,512,128]{2,0,1:T(4,128)}, u32[]{:S(2)}) copy-start(f32[4,512,128]{2,0,1:T(4,128)} %fusion.12) | copy-start | bytes 3145732
  41.8 2.5 %copy-start.2 = (f32[4,512,1,128]{3,1,2,0:T(8,128)S(1)}, f32[4,512,1,128]{3,1,2,0:T(8,128)}, u32[]{:S(2)}) copy-start(f32[4,512,1,128]{3,1,2,0:T(8,128)} %copy-done.1) | copy-start | bytes 3145732
  79.5 30.8 %all-to-all-start.2 = ((f32[8,64,4,1,128]{4,2,1,3,0:T(4,128)}), f32[8,64,4,1,128]{4,2,1,3,0:T(4,128)}, u32[]{:S(2)}, u32[]{:S(2)}) async-start(f32[8,64,4,1,128]{4,2,1,3,0:T(4,128)} %bitcast.201), calls=%async_computation.2 | async-start | bytes 2097152 | tf_op jit(solution)/shard_map/all_to_all | solution.py:70
  110.4 2.8 %copy-start.4 = (f32[8,64,4,128]{3,0,2,1:T(8,128)S(1)}, f32[8,64,4,128]{3,0,2,1:T(8,128)}, u32[]{:S(2)}) copy-start(f32[8,64,4,128]{3,0,2,1:T(8,128)} %fusion.8) | copy-start | bytes 3145732
  125.4 9.8 %copy-start.5 = (bf16[4,128,128]{2,1,0:T(8,128)(2,1)S(1)}, bf16[4,128,128]{2,1,0:T(8,128)(2,1)}, u32[]{:S(2)}) copy-start(bf16[4,128,128]{2,1,0:T(8,128)(2,1)} %param.4) | copy-start | bytes 393220
  131.7 18.8 %all-to-all-start.4 = ((bf16[8,1,64,1,4,1,128]{6,2,5,4,3,1,0:T(8,128)(2,1)}), bf16[8,1,64,1,4,1,128]{6,2,5,4,3,1,0:T(8,128)(2,1)S(1)}, u32[]{:S(2)}, u32[]{:S(2)}) async-start(bf16[8,1,64,1,4,1,128]{6,2,5,4,3,1,0:T(8,128)(2,1)} %copy.67), calls=%async_computation.4 | async-start | bytes 1048576 | tf_op jit(solution)/shard_map/all_to_all | solution.py:88
